TPU v7x, 32 devices: a whole 2x2x4 slice. The times are simulated.
32 devices in a mesh: fs: 4 (over z), rep: 4 (over y, x), tp: 2 (over core).
Axes of the slice: x: 2, y: 2, z: 4, core: 2. Of those that a mesh axis runs over, the one named last changes fastest.
Arguments:
- normed_input: bfloat16 [2048, 1024], P(('fs', 'rep')), may hold values from -6 to 6
- query_cotangent: bfloat16 [2048, 512], P(('fs', 'rep'), 'tp'), may hold values from -0.029907227 to 0.029907227
- value_cotangent: bfloat16 [2048, 1024], P(('fs', 'rep'), 'tp'), may hold values from -0.029907227 to 0.029907227
- query_basis: bfloat16 [1024, 128], replicated, may hold values from -0.1875 to 0.1875
- value_basis: bfloat16 [1024, 128], replicated, may hold values from -0.1875 to 0.1875
- query_weight: float32 [1024, 512], P(('fs', 'rep'), 'tp'), may hold values from -0.1875 to 0.1875
- value_weight: float32 [1024, 1024], P(('fs', 'rep'), 'tp'), may hold values from -0.1875 to 0.1875
- query_first: float32 [128, 512], P(('fs', 'rep'), 'tp'), may hold values from -6 to 6
- query_second: float32 [128, 512], P(('fs', 'rep'), 'tp'), may hold values from 0.25 to 4
- value_first: float32 [128, 1024], P(('fs', 'rep'), 'tp'), may hold values from -6 to 6
- value_second: float32 [128, 1024], P(('fs', 'rep'), 'tp'), may hold values from 0.25 to 4
Outputs:
- query_update: float32 [1024, 512], P(('fs', 'rep'), 'tp')
- value_update: float32 [1024, 1024], P(('fs', 'rep'), 'tp')
- query_weight_new: float32 [1024, 512], P(('fs', 'rep'), 'tp')
- value_weight_new: float32 [1024, 1024], P(('fs', 'rep'), 'tp')
- query_first_new: float32 [128, 512], P(('fs', 'rep'), 'tp')
- query_second_new: float32 [128, 512], P(('fs', 'rep'), 'tp')
- value_first_new: float32 [128, 1024], P(('fs', 'rep'), 'tp')
- value_second_new: float32 [128, 1024], P(('fs', 'rep'), 'tp')
- query_copy: bfloat16 [1024, 512], P(None, 'tp')
- value_copy: bfloat16 [1024, 1024], P(None, 'tp')
All inputs are finite; a program needn't handle non-finite values.
Results may differ from a plain program's by a relative error of at most 0.001.
Values may be sent and summed in bfloat16 or wider, within the bound.
A program may use at most 64 MiB of HBM per device.

v0:
```python
import jax
import jax.numpy as jnp
from jax import lax
from jax.sharding import PartitionSpec as P


def moments(projected, first_old, second_old):
    first_new = 0.9 * first_old + 0.1 * projected
    second_new = 0.99 * second_old + 0.01 * projected * projected
    return (first_new, second_new, first_new / (jnp.sqrt(second_new) + 1e-08))


def finish(whole_dir, basis_rows, weight, squares, entries):
    norm_scale = jnp.sqrt(squares / entries + 1.0)
    update = jnp.dot(basis_rows, whole_dir, precision=lax.Precision.HIGHEST) / norm_scale
    weight_new = weight - 0.01 * update
    return (update, weight_new, weight_new.astype(jnp.bfloat16))


def split_parts(reduced):
    high_part = reduced.astype(jnp.bfloat16)
    held = lax.optimization_barrier(high_part)
    low_part = (reduced - held.astype(jnp.float32)).astype(jnp.bfloat16)
    return (high_part, low_part)


def parts_product(high_part, low_part, cotangent):
    dims = (((0,), (0,)), ((), ()))
    first_term = lax.dot_general(high_part, cotangent, dims, preferred_element_type=jnp.float32)
    second_term = lax.dot_general(low_part, cotangent, dims, preferred_element_type=jnp.float32)
    return first_term + second_term


def body(
    normed_input,
    query_cotangent,
    value_cotangent,
    query_basis,
    value_basis,
    query_weight,
    value_weight,
    query_first,
    query_second,
    value_first,
    value_second,
):
    row_count = query_weight.shape[0]
    query_width = query_cotangent.shape[1]
    offset = lax.axis_index(("fs", "rep")) * row_count
    query_rows = lax.dynamic_slice_in_dim(query_basis, offset, row_count, 0).astype(jnp.float32)
    value_rows = lax.dynamic_slice_in_dim(value_basis, offset, row_count, 0).astype(jnp.float32)
    reduced_query = jnp.dot(normed_input, query_basis, preferred_element_type=jnp.float32)
    reduced_value = jnp.dot(normed_input, value_basis, preferred_element_type=jnp.float32)
    query_high, query_low = split_parts(reduced_query)
    value_high, value_low = split_parts(reduced_value)
    projected = lax.psum_scatter(
        jnp.concatenate(
            [
                parts_product(query_high, query_low, query_cotangent),
                parts_product(value_high, value_low, value_cotangent),
            ],
            axis=1,
        ),
        ("fs", "rep"),
        scatter_dimension=0,
        tiled=True,
    )
    query_projected = projected[:, :query_width]
    value_projected = projected[:, query_width:]
    query_first_new, query_second_new, query_dir = moments(
        query_projected, query_first, query_second
    )
    value_first_new, value_second_new, value_dir = moments(
        value_projected, value_first, value_second
    )
    query_whole, value_whole = (
        lax.all_gather(query_dir, ("fs", "rep"), axis=0, tiled=True),
        lax.all_gather(value_dir, ("fs", "rep"), axis=0, tiled=True),
    )
    query_squares, value_squares = lax.psum(
        (jnp.sum(query_dir * query_dir), jnp.sum(value_dir * value_dir)), ("fs", "rep", "tp")
    )
    tp_count = lax.axis_size("tp")
    query_update, query_weight_new, query_half = finish(
        query_whole,
        query_rows,
        query_weight,
        query_squares,
        query_whole.shape[0] * query_whole.shape[1] * tp_count,
    )
    value_update, value_weight_new, value_half = finish(
        value_whole,
        value_rows,
        value_weight,
        value_squares,
        value_whole.shape[0] * value_whole.shape[1] * tp_count,
    )
    query_copy, value_copy = (
        lax.all_gather(query_half, ("fs", "rep"), axis=0, tiled=True),
        lax.all_gather(value_half, ("fs", "rep"), axis=0, tiled=True),
    )
    return (
        query_update,
        value_update,
        query_weight_new,
        value_weight_new,
        query_first_new,
        query_second_new,
        value_first_new,
        value_second_new,
        query_copy,
        value_copy,
    )


def solution(mesh):
    in_specs = (
        P(("fs", "rep"), None),
        P(("fs", "rep"), "tp"),
        P(("fs", "rep"), "tp"),
        P(),
        P(),
        P(("fs", "rep"), "tp"),
        P(("fs", "rep"), "tp"),
        P(("fs", "rep"), "tp"),
        P(("fs", "rep"), "tp"),
        P(("fs", "rep"), "tp"),
        P(("fs", "rep"), "tp"),
    )
    out_specs = (
        P(("fs", "rep"), "tp"),
        P(("fs", "rep"), "tp"),
        P(("fs", "rep"), "tp"),
        P(("fs", "rep"), "tp"),
        P(("fs", "rep"), "tp"),
        P(("fs", "rep"), "tp"),
        P(("fs", "rep"), "tp"),
        P(("fs", "rep"), "tp"),
        P(None, "tp"),
        P(None, "tp"),
    )
    return jax.shard_map(body, mesh=mesh, in_specs=in_specs, out_specs=out_specs, check_vma=False)
```

profile of v0, /device:TPU:0, one launch (start us, length us, event | category | flops | bytes accessed | tf_op | source)
XLA Modules:
  0.0 313.8 jit_solution(15066968954675229272)
XLA Ops:
  7.2 0.0 copy-start
  7.2 0.0 copy-start.3
  7.2 0.0 reduce-scatter.2.cloned.1.call-start
  7.2 0.9 copy-done
  8.1 0.0 copy-start.4
  8.1 1.2 fusion.10
  9.3 0.0 copy-start.2
  9.4 0.0 copy-done.3
  9.4 0.2 fusion.13
  9.6 0.0 copy-done.4
  9.6 0.7 copy-done.2
  10.3 0.0 copy-start.5
  10.3 0.2 fusion.11
  10.5 0.6 copy-done.5
  11.1 0.2 fusion.12
  11.3 0.2 convolution_add_fusion
  11.6 0.2 convolution_add_fusion.1
  11.8 0.8 pad_maximum_fusion
  12.5 0.0 copy-start.9
  12.5 0.0 reduce-scatter.2.cloned.1.call-update
  12.6 0.0 copy-start.8
  12.6 0.0 all-gather.2.cloned.1.call-start
  12.6 0.0 copy-start.10
  12.6 0.0 copy-start.11
  12.7 126.3 %reduce-scatter.2.cloned.1.call-done = f32[8,768]{1,0:T(8,128)} async-done(((f32[128,768]{1,0:T(8,128)}), f32[8,768]{1,0:T(8,128)}) %reduce-scatter.2.cloned.1.call-update) | async-done | bytes 24592 | tf_op jit(solution)/shard_map/reduce_scatter | solution.py:56
  138.9 0.0 copy-done.9
  138.9 0.0 copy-done.8
  138.9 1.9 multiply_reduce_fusion
  140.9 0.0 copy-done.10
  140.9 0.0 copy-done.11
  140.9 1.9 multiply_reduce_fusion.1
  142.8 40.4 %all-reduce = (f32[]{:T(128)}, f32[]{:T(128)}) all-reduce(f32[]{:T(128)} %get-tuple-element.20, f32[]{:T(128)} %get-tuple-element.16), channel_id=1, replica_groups=mesh['fs'=4,'rep'=4,'tp'=2] {'fs','rep','tp'}, use_global_device_ids=true, to_apply=%region_2.0 | all-reduce | flops 2 | bytes 16 | tf_op jit(solution)/shard_map/psum | solution.py:80
  183.9 0.0 copy-start.6
  183.9 40.3 %all_gather.13 = f32[128,512]{1,0:T(8,128)S(1)} all-gather(f32[8,512]{1,0:T(8,128)S(1)} %get-tuple-element.17), channel_id=1, replica_groups=mesh['fs'=4,'rep'=4,'tp'=2] {'fs','rep'}, dimensions={0}, use_global_device_ids=true | all-gather | bytes 278528 | tf_op jit(solution)/shard_map/all_gather | solution.py:78
  224.2 0.0 copy-done.6
  224.2 1.0 fusion.6
  225.2 0.0 all-gather.2.cloned.1.call-update
  225.9 0.0 copy-start.7
  225.9 36.5 %all_gather.12 = f32[128,256]{1,0:T(8,128)S(1)} all-gather(f32[8,256]{1,0:T(8,128)S(1)} %get-tuple-element.21), channel_id=1, replica_groups=mesh['fs'=4,'rep'=4,'tp'=2] {'fs','rep'}, dimensions={0}, use_global_device_ids=true | all-gather | bytes 139264 | tf_op jit(solution)/shard_map/all_gather | solution.py:77
  262.3 0.0 copy-done.7
  262.3 0.8 fusion.7
  263.2 41.4 %all_gather.14 = bf16[1024,256]{1,0:T(8,128)(2,1)S(1)} all-gather(bf16[64,256]{1,0:T(8,128)(2,1)S(1)} %get-tuple-element.14), channel_id=1, replica_groups=mesh['fs'=4,'rep'=4,'tp'=2] {'fs','rep'}, dimensions={0}, use_global_device_ids=true | all-gather | bytes 557056 | tf_op jit(solution)/shard_map/all_gather | solution.py:99
  304.5 0.0 all-gather.2.cloned.1.call-done
  304.5 0.0 copy-start.1
  304.5 0.8 copy.23
  305.3 0.6 copy-done.1
  306.0 1.0 copy.24
Async XLA Ops:
  7.2 1.0 copy-start
  7.2 2.2 copy-start.3
  7.2 131.7 %reduce-scatter.2.cloned.1.call-start = ((), (), s32[]{:S(2)}) async-start(), calls=%async_computation.1 | async-start | bytes 417792 | tf_op jit(solution)/shard_map/reduce_scatter | solution.py:56
  8.1 1.5 copy-start.4
  9.3 1.0 copy-start.2
  10.3 0.8 copy-start.5
  12.5 126.4 %copy-start.9 = (f32[8,512]{1,0:T(8,128)S(1)}, f32[8,512]{1,0:T(8,128)}, u32[]{:S(2)}) copy-start(f32[8,512]{1,0:T(8,128)} %param.20) | copy-start | bytes 49156
  12.6 126.4 %copy-start.8 = (f32[8,512]{1,0:T(8,128)S(1)}, f32[8,512]{1,0:T(8,128)}, u32[]{:S(2)}) copy-start(f32[8,512]{1,0:T(8,128)} %param.21) | copy-start | bytes 49156
  12.6 292.0 %all-gather.2.cloned.1.call-start = ((), (), s32[]{:S(2)}) async-start(), calls=%async_computation.2 | async-start | bytes 1114112 | tf_op jit(solution)/shard_map/all_gather | solution.py:100
  12.6 128.2 %copy-start.10 = (f32[8,256]{1,0:T(8,128)S(1)}, f32[8,256]{1,0:T(8,128)}, u32[]{:S(2)}) copy-start(f32[8,256]{1,0:T(8,128)} %param.19) | copy-start | bytes 24580
  12.6 128.2 %copy-start.11 = (f32[8,256]{1,0:T(8,128)S(1)}, f32[8,256]{1,0:T(8,128)}, u32[]{:S(2)}) copy-start(f32[8,256]{1,0:T(8,128)} %param.18) | copy-start | bytes 24580
  183.9 40.3 %copy-start.6 = (f32[64,512]{1,0:T(8,128)S(1)}, f32[64,512]{1,0:T(8,128)}, u32[]{:S(2)}) copy-start(f32[64,512]{1,0:T(8,128)} %param.17) | copy-start | bytes 393220
  225.9 36.5 %copy-start.7 = (f32[64,256]{1,0:T(8,128)S(1)}, f32[64,256]{1,0:T(8,128)}, u32[]{:S(2)}) copy-start(f32[64,256]{1,0:T(8,128)} %param.16) | copy-start | bytes 196612
  304.5 1.4 copy-start.1
Sparse Core Ops, SparseCore 0:
  13.2 125.6 reduce-scatter.1
  225.3 52.1 all-gather.1
where the time goes:
time: 314 us
  blocking collectives  159 us (51%)
  waiting for transfers between devices  126 us (40%)
  between operations  15.6 us (5%)
  local copies, waits for them, and re-layouts  4.65 us (1%)
  other arithmetic  4.61 us (1%)
  matrix products  4.03 us (1%)
    reduce_scatter x1, waiting for transfers between devices, body(): lax.psum_scatter(jnp.concatenate([parts_product(query_high, query_low, qu...  126 us
    all_gather x1, blocking collectives, body(): lax.all_gather(query_half, ('fs', 'rep'), axis=0, tiled=True)  41.4 us
    psum x1, blocking collectives, body(): lax.psum((jnp.sum(query_dir * query_dir), jnp.sum(value_dir * value_dir))...  40.4 us
    all_gather x1, blocking collectives, body(): lax.all_gather(value_dir, ('fs', 'rep'), axis=0, tiled=True)  40.3 us
    all_gather x1, blocking collectives, body(): lax.all_gather(query_dir, ('fs', 'rep'), axis=0, tiled=True)  36.5 us
  transfers between devices with their start and end apart: 2, of which 1 were waited for; matrix products, arithmetic and copies ran while one was open for 0% of the time, Pallas kernels for 0%

commit v1 on v0

--- a/solution.py
+++ b/solution.py
@@ -1,6 +1,9 @@
+import functools
 import jax
 import jax.numpy as jnp
 from jax import lax
+from jax.experimental import pallas as pl
+from jax.experimental.pallas import tpu as pltpu
 from jax.sharding import PartitionSpec as P
 
 
@@ -113,6 +116,233 @@
     )
 
 
+MESH = pl.DeviceIdType.MESH
+f32, bf16 = jnp.float32, jnp.bfloat16
+
+
+def two_parts(x):
+    high = x.astype(bf16)
+    return high, (x - high.astype(f32)).astype(bf16)
+
+
+def three_parts(x):
+    high = x.astype(bf16)
+    rest = x - high.astype(f32)
+    middle = rest.astype(bf16)
+    return high, middle, (rest - middle.astype(f32)).astype(bf16)
+
+
+def remote(src, dst, sems, index, peer):
+    return pltpu.make_async_remote_copy(
+        src_ref=src,
+        dst_ref=dst,
+        send_sem=sems[0].at[index],
+        recv_sem=sems[1].at[index],
+        device_id=peer,
+        device_id_type=MESH,
+    )
+
+
+def kernel(
+    F, R, T,
+    x_ref, qc_ref, vc_ref, qb_ref, vb_ref, qw_ref, vw_ref, qf_ref, qs_ref, vf_ref, vs_ref,
+    qu_ref, vu_ref, qn_ref, vn_ref, qfn_ref, qsn_ref, vfn_ref, vsn_ref, qcopy_ref, vcopy_ref,
+    part, got1, mid, got2, dirs, squares, squares_in,
+    s1, r1, s2, r2, s3, r3, s4, r4, s5, r5, s6, r6, s7, r7,
+):
+    z, r, t = lax.axis_index("fs"), lax.axis_index("rep"), lax.axis_index("tp")
+    zs = [lax.rem(z + k, F) for k in range(F)]
+    rs = [lax.rem(r + k, R) for k in range(R)]
+    ts = [lax.rem(t + k, T) for k in range(T)]
+    back = [lax.rem(z + F - k, F) for k in range(F)]
+    rows = qw_ref.shape[0]
+    QC, VC = qc_ref.shape[1], vc_ref.shape[1]
+    M = qf_ref.shape[0]
+
+    barrier = pltpu.get_barrier_semaphore()
+    for axis, others in (("rep", rs), ("fs", zs), ("tp", ts)):
+        for other in others[1:]:
+            pl.semaphore_signal(barrier, inc=1, device_id={axis: other}, device_id_type=MESH)
+
+    x = x_ref[...]
+    for basis, cot, start, width in ((qb_ref, qc_ref, 0, QC), (vb_ref, vc_ref, QC, VC)):
+        reduced = jnp.dot(x, basis[...], preferred_element_type=f32).T
+        high, low = two_parts(reduced)
+        c = cot[...]
+        total = jnp.dot(high, c, preferred_element_type=f32) + jnp.dot(
+            low, c, preferred_element_type=f32
+        )
+        for a in range(F):
+            for b in range(R):
+                at = (a * R + b) * M
+                part[b, a, :, start : start + width] = total[at : at + M]
+
+    pl.semaphore_wait(barrier, F + R + T - 3)
+
+    sends = []
+    first = [remote(part.at[rs[k]], got1.at[k], (s1, r1), k, {"rep": rs[k]}) for k in range(1, R)]
+    for c in first:
+        c.start()
+    sends += first
+    for c in first:
+        c.wait_recv()
+    total = part[r]
+    for k in range(1, R):
+        total = total + got1[k]
+    mid[...] = total
+    second = [remote(mid.at[zs[k]], got2.at[k], (s2, r2), k, {"fs": zs[k]}) for k in range(1, F)]
+    for c in second:
+        c.start()
+    sends += second
+    projected = mid[z]
+    for k in range(1, F):
+        second[k - 1].wait_recv()
+        projected = projected + got2[k]
+
+    for f_ref, s_ref, fn_ref, sn_ref, start, width in (
+        (qf_ref, qs_ref, qfn_ref, qsn_ref, 0, QC),
+        (vf_ref, vs_ref, vfn_ref, vsn_ref, QC, VC),
+    ):
+        p = projected[:, start : start + width]
+        fn = 0.9 * f_ref[...] + 0.1 * p
+        sn = 0.99 * s_ref[...] + 0.01 * p * p
+        fn_ref[...] = fn
+        sn_ref[...] = sn
+        dirs[z, r, :, start : start + width] = fn / (jnp.sqrt(sn) + 1e-08)
+
+    third = [remote(dirs.at[z, r], dirs.at[z, r], (s3, r3), k, {"fs": zs[k]}) for k in range(1, F)]
+    for c in third:
+        c.start()
+    sends += third
+    fourth = []
+    for j in range(F):
+        if j > 0:
+            third[j - 1].wait_recv()
+        block = dirs.at[back[j], r]
+        for k in range(1, R):
+            c = remote(block, block, (s4, r4), (j, k), {"rep": rs[k]})
+            c.start()
+            fourth.append(c)
+    sends += fourth
+    for c in fourth:
+        c.wait_recv()
+
+    whole = dirs[...].reshape(F * R * M, QC + VC)
+    for i, (start, width) in enumerate(((0, QC), (QC, VC))):
+        d = whole[:, start : start + width]
+        d = (d * d).reshape(F * R * M // 8, 8, width).sum(axis=0)
+        acc = d[:, :128]
+        for b in range(1, width // 128):
+            acc = acc + d[:, b * 128 : (b + 1) * 128]
+        squares[i] = acc
+    fifth = [remote(squares, squares_in.at[k], (s5, r5), k, {"tp": ts[k]}) for k in range(1, T)]
+    for c in fifth:
+        c.start()
+    sends += fifth
+
+    offset = pl.multiple_of((z * R + r) * rows, rows)
+    raw = []
+    for basis, start, width in ((qb_ref, 0, QC), (vb_ref, QC, VC)):
+        b = basis[pl.ds(offset, rows), :]
+        d1, d2, d3 = three_parts(whole[:, start : start + width])
+        raw.append(
+            jnp.dot(b, d1, preferred_element_type=f32)
+            + (jnp.dot(b, d2, preferred_element_type=f32) + jnp.dot(b, d3, preferred_element_type=f32))
+        )
+    for c in fifth:
+        c.wait_recv()
+    sq = squares[...]
+    for k in range(1, T):
+        sq = sq + squares_in[k]
+    for i, (w_ref, u_ref, n_ref, copy_ref, width) in enumerate((
+        (qw_ref, qu_ref, qn_ref, qcopy_ref, QC),
+        (vw_ref, vu_ref, vn_ref, vcopy_ref, VC),
+    )):
+        scale = jnp.sqrt(jnp.sum(sq[i], keepdims=True) / (F * R * M * width * T) + 1.0)
+        update = raw[i] / scale
+        new = w_ref[...] - 0.01 * update
+        u_ref[...] = update
+        n_ref[...] = new
+        copy_ref[pl.ds(offset, rows), :] = new.astype(bf16)
+
+    sixth = []
+    for k in range(1, F):
+        for i, ref in enumerate((qcopy_ref, vcopy_ref)):
+            own = ref.at[pl.ds(offset, rows), :]
+            c = remote(own, own, (s6, r6), (k, i), {"fs": zs[k]})
+            c.start()
+            sixth.append(c)
+    sends += sixth
+    seventh = []
+    for j in range(F):
+        at = pl.multiple_of((back[j] * R + r) * rows, rows)
+        for i, ref in enumerate((qcopy_ref, vcopy_ref)):
+            if j > 0:
+                sixth[(j - 1) * 2 + i].wait_recv()
+            block = ref.at[pl.ds(at, rows), :]
+            for k in range(1, R):
+                c = remote(block, block, (s7, r7), (j, k * 2 + i), {"rep": rs[k]})
+                c.start()
+                seventh.append(c)
+    sends += seventh
+    for c in seventh:
+        c.wait_recv()
+    for c in sends:
+        c.wait_send()
+
+
+def fused(plain, *args):
+    x, qc, vc, qb, vb, qw, vw, qf, qs, vf, vs = args
+    F, R, T = (lax.axis_size(name) for name in ("fs", "rep", "tp"))
+    QC, VC = qc.shape[1], vc.shape[1]
+    M, rows = qf.shape[0], qw.shape[0]
+    aligned = M % 8 == 0 and rows % 16 == 0 and QC % 128 == 0 and VC % 128 == 0
+    if not aligned:
+        return plain(*args)
+    W = QC + VC
+    out = jax.ShapeDtypeStruct
+    vmem = pl.BlockSpec(memory_space=pltpu.VMEM)
+    dma = pltpu.SemaphoreType.DMA
+    return tuple(
+        pl.pallas_call(
+            functools.partial(kernel, F, R, T),
+            out_shape=[
+                out(qw.shape, f32),
+                out(vw.shape, f32),
+                out(qw.shape, f32),
+                out(vw.shape, f32),
+                out(qf.shape, f32),
+                out(qf.shape, f32),
+                out(vf.shape, f32),
+                out(vf.shape, f32),
+                out((rows * F * R, QC), bf16),
+                out((rows * F * R, VC), bf16),
+            ],
+            in_specs=[vmem] * 11,
+            out_specs=[vmem] * 10,
+            scratch_shapes=[
+                pltpu.VMEM((R, F, M, W), f32),
+                pltpu.VMEM((R, F, M, W), f32),
+                pltpu.VMEM((F, M, W), f32),
+                pltpu.VMEM((F, M, W), f32),
+                pltpu.VMEM((F, R, M, W), f32),
+                pltpu.VMEM((2, 8, 128), f32),
+                pltpu.VMEM((T, 2, 8, 128), f32),
+                dma((R,)), dma((R,)),
+                dma((F,)), dma((F,)),
+                dma((F,)), dma((F,)),
+                dma((F, R)), dma((F, R)),
+                dma((T,)), dma((T,)),
+                dma((F, 2)), dma((F, 2)),
+                dma((F, 2 * R)), dma((F, 2 * R)),
+            ],
+            compiler_params=pltpu.CompilerParams(
+                collective_id=0, has_side_effects=True, vmem_limit_bytes=48 * 2**20
+            ),
+        )(*args)
+    )
+
+
 def solution(mesh):
     in_specs = (
         P(("fs", "rep"), None),
@@ -139,4 +369,4 @@
         P(None, "tp"),
         P(None, "tp"),
     )
-    return jax.shard_map(body, mesh=mesh, in_specs=in_specs, out_specs=out_specs, check_vma=False)
+    return jax.shard_map(functools.partial(fused, body), mesh=mesh, in_specs=in_specs, out_specs=out_specs, check_vma=False)

time: 314 us -> 62.5 us (0.20)
  blocking collectives: 159 us -> 0 us
  waiting for transfers between devices: 126 us -> 0 us
  Pallas kernels: 0 us -> 45.4 us
  between operations: 15.6 us -> 0.68 us
  local copies, waits for them, and re-layouts: 4.65 us -> 15.9 us
  other arithmetic: 4.61 us -> 0 us
  matrix products: 4.03 us -> 0 us
    reduce_scatter x1 -> x0, waiting for transfers between devices: 126 us -> none  [body(): lax.psum_scatter(jnp.concatenate([parts_product(query_high, query_low, qu...]
    all_gather x3 -> x0, blocking collectives: 118 us -> none  [the longest x1 41.4 us: body(): lax.all_gather(query_half, ('fs', 'rep'), axis=0, tiled=True)]
    pallas_call x0 -> x1, Pallas kernels: none -> 45.4 us  [fused(): pl.pallas_call(functools.partial(kernel, F, R, T), out_shape=[out(qw.shap...]
    psum x1 -> x0, blocking collectives: 40.4 us -> none  [body(): lax.psum((jnp.sum(query_dir * query_dir), jnp.sum(value_dir * value_dir))...]
    unnamed x26 -> x32, local copies, waits for them, and re-layouts: 4.65 us -> 15.9 us
    dot_general x8 -> x0, matrix products: 4.03 us -> none  [the longest x2 1.8 us: finish(): jnp.dot(basis_rows, whole_dir, precision=lax.Precision.HIGHEST) / norm_scale]
    reduce_sum x2 -> x0, other arithmetic: 3.83 us -> none  [the longest x1 1.93 us: body(): jnp.sum(value_dir * value_dir)]
  transfers between devices with their start and end apart: 2 -> 0, of which waited for: 1 -> 0; matrix products, arithmetic and copies ran while one was open for 0% -> 0% of each run, Pallas kernels for 0% -> 0%
where the time goes in v1:
time: 62.5 us; the launch traced here: 62 us
  Pallas kernels  45.4 us (73%)
  local copies, waits for them, and re-layouts  15.9 us (25%)
  between operations  0.68 us (1%)
    pallas_call x1, Pallas kernels, fused(): pl.pallas_call(functools.partial(kernel, F, R, T), out_shape=[out(qw.shap...  45.4 us
    unnamed x32, local copies, waits for them, and re-layouts  15.9 us

profile of v1, /device:TPU:0, one launch (start us, length us, event | category | flops | bytes accessed | tf_op | source)
XLA Modules:
  0.0 62.0 jit_solution(8140001982237254379)
XLA Ops:
  0.6 0.0 copy-start
  0.7 0.9 %copy-done = bf16[128,1024]{1,0:T(8,128)(2,1)S(1)} copy-done((bf16[128,1024]{1,0:T(8,128)(2,1)S(1)}, bf16[128,1024]{1,0:T(8,128)(2,1)}, u32[]{:S(2)}) %copy-start) | copy-done | bytes 262168
  1.6 0.0 copy-start.1
  1.6 0.9 %copy-done.1 = bf16[1024,128]{1,0:T(8,128)(2,1)S(1)} copy-done((bf16[1024,128]{1,0:T(8,128)(2,1)S(1)}, bf16[1024,128]{1,0:T(8,128)(2,1)}, u32[]{:S(2)}) %copy-start.1) | copy-done | bytes 262168
  2.5 0.0 copy-start.2
  2.6 0.9 %copy-done.2 = bf16[1024,128]{1,0:T(8,128)(2,1)S(1)} copy-done((bf16[1024,128]{1,0:T(8,128)(2,1)S(1)}, bf16[1024,128]{1,0:T(8,128)(2,1)}, u32[]{:S(2)}) %copy-start.2) | copy-done | bytes 262168
  3.5 0.0 copy-start.3
  3.5 0.9 %copy-done.3 = bf16[128,512]{1,0:T(8,128)(2,1)S(1)} copy-done((bf16[128,512]{1,0:T(8,128)(2,1)S(1)}, bf16[128,512]{1,0:T(8,128)(2,1)}, u32[]{:S(2)}) %copy-start.3) | copy-done | bytes 131096
  4.4 0.0 copy-start.4
  4.4 0.9 %copy-done.4 = f32[64,512]{1,0:T(8,128)S(1)} copy-done((f32[64,512]{1,0:T(8,128)S(1)}, f32[64,512]{1,0:T(8,128)}, u32[]{:S(2)}) %copy-start.4) | copy-done | bytes 131096
  5.3 0.0 copy-start.5
  5.3 0.8 %copy-done.5 = bf16[128,256]{1,0:T(8,128)(2,1)S(1)} copy-done((bf16[128,256]{1,0:T(8,128)(2,1)S(1)}, bf16[128,256]{1,0:T(8,128)(2,1)}, u32[]{:S(2)}) %copy-start.5) | copy-done | bytes 65560
  6.1 0.0 copy-start.6
  6.2 0.8 %copy-done.6 = f32[64,256]{1,0:T(8,128)S(1)} copy-done((f32[64,256]{1,0:T(8,128)S(1)}, f32[64,256]{1,0:T(8,128)}, u32[]{:S(2)}) %copy-start.6) | copy-done | bytes 65560
  7.0 0.0 copy-start.7
  7.0 0.7 %copy-done.7 = f32[8,512]{1,0:T(8,128)S(1)} copy-done((f32[8,512]{1,0:T(8,128)S(1)}, f32[8,512]{1,0:T(8,128)}, u32[]{:S(2)}) %copy-start.7) | copy-done | bytes 16408
  7.7 0.0 copy-start.8
  7.7 0.7 %copy-done.8 = f32[8,512]{1,0:T(8,128)S(1)} copy-done((f32[8,512]{1,0:T(8,128)S(1)}, f32[8,512]{1,0:T(8,128)}, u32[]{:S(2)}) %copy-start.8) | copy-done | bytes 16408
  8.4 0.0 copy-start.9
  8.4 0.7 %copy-done.9 = f32[8,256]{1,0:T(8,128)S(1)} copy-done((f32[8,256]{1,0:T(8,128)S(1)}, f32[8,256]{1,0:T(8,128)}, u32[]{:S(2)}) %copy-start.9) | copy-done | bytes 8216
  9.1 0.0 copy-start.10
  9.1 0.7 %copy-done.10 = f32[8,256]{1,0:T(8,128)S(1)} copy-done((f32[8,256]{1,0:T(8,128)S(1)}, f32[8,256]{1,0:T(8,128)}, u32[]{:S(2)}) %copy-start.10) | copy-done | bytes 8216
  9.8 45.4 %shard_map.186 = (f32[64,256]{1,0:T(8,128)S(1)}, f32[64,512]{1,0:T(8,128)S(1)}, f32[64,256]{1,0:T(8,128)S(1)}, f32[64,512]{1,0:T(8,128)S(1)}, f32[8,256]{1,0:T(8...) custom-call(bf16[128,1024]{1,0:T(8,128)(2,1)S(1)} %copy-done, ...), custom_call_target="tpu_custom_call" | custom-call | tf_op jit(solution)/shard_map/pallas_call | solution.py:307
  55.2 0.6 %copy.31 = f32[64,256]{1,0:T(8,128)} copy(f32[64,256]{1,0:T(8,128)S(1)} %get-tuple-element.20) | data formatting | bytes 131072
  55.9 0.7 %copy.32 = f32[64,512]{1,0:T(8,128)} copy(f32[64,512]{1,0:T(8,128)S(1)} %get-tuple-element.21) | data formatting | bytes 262144
  56.5 0.6 %copy.33 = f32[64,256]{1,0:T(8,128)} copy(f32[64,256]{1,0:T(8,128)S(1)} %get-tuple-element.22) | data formatting | bytes 131072
  57.1 0.7 %copy.34 = f32[64,512]{1,0:T(8,128)} copy(f32[64,512]{1,0:T(8,128)S(1)} %get-tuple-element.23) | data formatting | bytes 262144
  57.8 0.6 copy.35
  58.4 0.6 copy.36
  59.0 0.6 copy.37
  59.6 0.6 copy.38
  60.2 0.8 %copy.39 = bf16[1024,256]{1,0:T(8,128)(2,1)} copy(bf16[1024,256]{1,0:T(8,128)(2,1)S(1)} %get-tuple-element.28) | data formatting | bytes 1048576
  61.0 1.0 %copy.40 = bf16[1024,512]{1,0:T(8,128)(2,1)} copy(bf16[1024,512]{1,0:T(8,128)(2,1)S(1)} %get-tuple-element.29) | data formatting | bytes 2097152
Async XLA Ops:
  0.6 1.0 %copy-start = (bf16[128,1024]{1,0:T(8,128)(2,1)S(1)}, bf16[128,1024]{1,0:T(8,128)(2,1)}, u32[]{:S(2)}) copy-start(bf16[128,1024]{1,0:T(8,128)(2,1)} %x_ref.1) | copy-start | bytes 786436
  1.6 0.9 %copy-start.1 = (bf16[1024,128]{1,0:T(8,128)(2,1)S(1)}, bf16[1024,128]{1,0:T(8,128)(2,1)}, u32[]{:S(2)}) copy-start(bf16[1024,128]{1,0:T(8,128)(2,1)} %qb_ref.1) | copy-start | bytes 786436
  2.5 0.9 %copy-start.2 = (bf16[1024,128]{1,0:T(8,128)(2,1)S(1)}, bf16[1024,128]{1,0:T(8,128)(2,1)}, u32[]{:S(2)}) copy-start(bf16[1024,128]{1,0:T(8,128)(2,1)} %vb_ref.1) | copy-start | bytes 786436
  3.5 0.9 %copy-start.3 = (bf16[128,512]{1,0:T(8,128)(2,1)S(1)}, bf16[128,512]{1,0:T(8,128)(2,1)}, u32[]{:S(2)}) copy-start(bf16[128,512]{1,0:T(8,128)(2,1)} %vc_ref.1) | copy-start | bytes 393220
  4.4 0.9 %copy-start.4 = (f32[64,512]{1,0:T(8,128)S(1)}, f32[64,512]{1,0:T(8,128)}, u32[]{:S(2)}) copy-start(f32[64,512]{1,0:T(8,128)} %vw_ref.1) | copy-start | bytes 393220
  5.3 0.8 %copy-start.5 = (bf16[128,256]{1,0:T(8,128)(2,1)S(1)}, bf16[128,256]{1,0:T(8,128)(2,1)}, u32[]{:S(2)}) copy-start(bf16[128,256]{1,0:T(8,128)(2,1)} %qc_ref.1) | copy-start | bytes 196612
  6.1 0.8 %copy-start.6 = (f32[64,256]{1,0:T(8,128)S(1)}, f32[64,256]{1,0:T(8,128)}, u32[]{:S(2)}) copy-start(f32[64,256]{1,0:T(8,128)} %qw_ref.1) | copy-start | bytes 196612
  7.0 0.7 %copy-start.7 = (f32[8,512]{1,0:T(8,128)S(1)}, f32[8,512]{1,0:T(8,128)}, u32[]{:S(2)}) copy-start(f32[8,512]{1,0:T(8,128)} %vf_ref.1) | copy-start | bytes 49156
  7.7 0.7 %copy-start.8 = (f32[8,512]{1,0:T(8,128)S(1)}, f32[8,512]{1,0:T(8,128)}, u32[]{:S(2)}) copy-start(f32[8,512]{1,0:T(8,128)} %vs_ref.1) | copy-start | bytes 49156
  8.4 0.7 %copy-start.9 = (f32[8,256]{1,0:T(8,128)S(1)}, f32[8,256]{1,0:T(8,128)}, u32[]{:S(2)}) copy-start(f32[8,256]{1,0:T(8,128)} %qf_ref.1) | copy-start | bytes 24580
  9.1 0.7 %copy-start.10 = (f32[8,256]{1,0:T(8,128)S(1)}, f32[8,256]{1,0:T(8,128)}, u32[]{:S(2)}) copy-start(f32[8,256]{1,0:T(8,128)} %qs_ref.1) | copy-start | bytes 24580

commit v2 on v1

--- a/solution.py
+++ b/solution.py
@@ -117,6 +117,8 @@
 
 
 MESH = pl.DeviceIdType.MESH
+VMEM_LIMIT = 60 * 2**20
+OUT_LIMIT = 16 * 2**20
 f32, bf16 = jnp.float32, jnp.bfloat16
 
 
@@ -145,27 +147,53 @@
 
 def kernel(
     F, R, T,
-    x_ref, qc_ref, vc_ref, qb_ref, vb_ref, qw_ref, vw_ref, qf_ref, qs_ref, vf_ref, vs_ref,
-    qu_ref, vu_ref, qn_ref, vn_ref, qfn_ref, qsn_ref, vfn_ref, vsn_ref, qcopy_ref, vcopy_ref,
+    x_hbm, qc_hbm, vc_hbm, qb_hbm, vb_hbm, qw_hbm, vw_hbm, qf_hbm, qs_hbm, vf_hbm, vs_hbm,
+    u_ref, n_ref, fn_ref, sn_ref, copy_ref,
+    x_ref, qc_ref, vc_ref, qb_ref, vb_ref, w_ref, f_ref, s_ref,
     part, got1, mid, got2, dirs, squares, squares_in,
-    s1, r1, s2, r2, s3, r3, s4, r4, s5, r5, s6, r6, s7, r7,
+    load, s1, r1, s2, r2, s3, r3, s4, r4, s5, r5, s6, r6, s7, r7,
 ):
     z, r, t = lax.axis_index("fs"), lax.axis_index("rep"), lax.axis_index("tp")
     zs = [lax.rem(z + k, F) for k in range(F)]
     rs = [lax.rem(r + k, R) for k in range(R)]
     ts = [lax.rem(t + k, T) for k in range(T)]
     back = [lax.rem(z + F - k, F) for k in range(F)]
-    rows = qw_ref.shape[0]
-    QC, VC = qc_ref.shape[1], vc_ref.shape[1]
-    M = qf_ref.shape[0]
+    rows = qw_hbm.shape[0]
+    QC, VC = qc_hbm.shape[1], vc_hbm.shape[1]
+    M = qf_hbm.shape[0]
 
     barrier = pltpu.get_barrier_semaphore()
     for axis, others in (("rep", rs), ("fs", zs), ("tp", ts)):
         for other in others[1:]:
             pl.semaphore_signal(barrier, inc=1, device_id={axis: other}, device_id_type=MESH)
 
+    query, value = pl.ds(0, QC), pl.ds(QC, VC)
+    loads = [
+        pltpu.make_async_copy(src, dst, load.at[i])
+        for i, (src, dst) in enumerate((
+            (x_hbm, x_ref),
+            (qb_hbm, qb_ref),
+            (qc_hbm, qc_ref),
+            (vb_hbm, vb_ref),
+            (vc_hbm, vc_ref),
+            (qf_hbm, f_ref.at[:, query]),
+            (vf_hbm, f_ref.at[:, value]),
+            (qs_hbm, s_ref.at[:, query]),
+            (vs_hbm, s_ref.at[:, value]),
+            (qw_hbm, w_ref.at[:, query]),
+            (vw_hbm, w_ref.at[:, value]),
+        ))
+    ]
+    for c in loads:
+        c.start()
+
+    loads[0].wait()
     x = x_ref[...]
-    for basis, cot, start, width in ((qb_ref, qc_ref, 0, QC), (vb_ref, vc_ref, QC, VC)):
+    for i, (basis, cot, start, width) in enumerate(
+        ((qb_ref, qc_ref, 0, QC), (vb_ref, vc_ref, QC, VC))
+    ):
+        loads[1 + 2 * i].wait()
+        loads[2 + 2 * i].wait()
         reduced = jnp.dot(x, basis[...], preferred_element_type=f32).T
         high, low = two_parts(reduced)
         c = cot[...]
@@ -180,35 +208,38 @@
     pl.semaphore_wait(barrier, F + R + T - 3)
 
     sends = []
-    first = [remote(part.at[rs[k]], got1.at[k], (s1, r1), k, {"rep": rs[k]}) for k in range(1, R)]
-    for c in first:
-        c.start()
-    sends += first
-    for c in first:
-        c.wait_recv()
-    total = part[r]
-    for k in range(1, R):
-        total = total + got1[k]
-    mid[...] = total
-    second = [remote(mid.at[zs[k]], got2.at[k], (s2, r2), k, {"fs": zs[k]}) for k in range(1, F)]
-    for c in second:
-        c.start()
-    sends += second
-    projected = mid[z]
-    for k in range(1, F):
-        second[k - 1].wait_recv()
-        projected = projected + got2[k]
-
-    for f_ref, s_ref, fn_ref, sn_ref, start, width in (
-        (qf_ref, qs_ref, qfn_ref, qsn_ref, 0, QC),
-        (vf_ref, vs_ref, vfn_ref, vsn_ref, QC, VC),
-    ):
-        p = projected[:, start : start + width]
-        fn = 0.9 * f_ref[...] + 0.1 * p
-        sn = 0.99 * s_ref[...] + 0.01 * p * p
-        fn_ref[...] = fn
-        sn_ref[...] = sn
-        dirs[z, r, :, start : start + width] = fn / (jnp.sqrt(sn) + 1e-08)
+    order = list(range(1, F)) + [0]
+    first = {
+        (j, k): remote(
+            part.at[rs[k], zs[j]], got1.at[k, j], (s1, r1), (j, k), {"rep": rs[k]}
+        )
+        for j in order
+        for k in range(1, R)
+    }
+    for c in first.values():
+        c.start()
+    sends += list(first.values())
+    second = {}
+    for j in order:
+        total = part[r, zs[j]]
+        for k in range(1, R):
+            first[j, k].wait_recv()
+            total = total + got1[k, j]
+        if j > 0:
+            mid[j] = total
+            second[j] = remote(mid.at[j], got2.at[j], (s2, r2), j, {"fs": zs[j]})
+            second[j].start()
+    sends += list(second.values())
+    for c in loads[5:]:
+        c.wait()
+    projected = total
+    for j in range(1, F):
+        second[j].wait_recv()
+        projected = projected + got2[j]
+
+    fn = 0.9 * f_ref[...] + 0.1 * projected
+    sn = 0.99 * s_ref[...] + 0.01 * projected * projected
+    dirs[z, r] = fn / (jnp.sqrt(sn) + 1e-08)
 
     third = [remote(dirs.at[z, r], dirs.at[z, r], (s3, r3), k, {"fs": zs[k]}) for k in range(1, F)]
     for c in third:
@@ -223,6 +254,9 @@
             c = remote(block, block, (s4, r4), (j, k), {"rep": rs[k]})
             c.start()
             fourth.append(c)
+        if j == 0:
+            fn_ref[...] = fn
+            sn_ref[...] = sn
     sends += fourth
     for c in fourth:
         c.wait_recv()
@@ -254,41 +288,86 @@
     sq = squares[...]
     for k in range(1, T):
         sq = sq + squares_in[k]
-    for i, (w_ref, u_ref, n_ref, copy_ref, width) in enumerate((
-        (qw_ref, qu_ref, qn_ref, qcopy_ref, QC),
-        (vw_ref, vu_ref, vn_ref, vcopy_ref, VC),
-    )):
+    for i, (start, width) in enumerate(((0, QC), (QC, VC))):
         scale = jnp.sqrt(jnp.sum(sq[i], keepdims=True) / (F * R * M * width * T) + 1.0)
         update = raw[i] / scale
-        new = w_ref[...] - 0.01 * update
-        u_ref[...] = update
-        n_ref[...] = new
-        copy_ref[pl.ds(offset, rows), :] = new.astype(bf16)
-
-    sixth = []
-    for k in range(1, F):
-        for i, ref in enumerate((qcopy_ref, vcopy_ref)):
-            own = ref.at[pl.ds(offset, rows), :]
-            c = remote(own, own, (s6, r6), (k, i), {"fs": zs[k]})
-            c.start()
-            sixth.append(c)
+        new = w_ref[:, start : start + width] - 0.01 * update
+        copy_ref[pl.ds(offset, rows), start : start + width] = new.astype(bf16)
+        u_ref[:, start : start + width] = update
+        n_ref[:, start : start + width] = new
+
+    own = copy_ref.at[pl.ds(offset, rows), :]
+    sixth = [remote(own, own, (s6, r6), k, {"fs": zs[k]}) for k in range(1, F)]
+    for c in sixth:
+        c.start()
     sends += sixth
-    seventh = []
+
+    def block_of(j, rep, first_row, count):
+        at = pl.multiple_of((back[j] * R + rep) * rows + first_row, count)
+        return copy_ref.at[pl.ds(at, count), :]
+
+    last = []
+    split = R == 4 and rows % 32 == 0
+    if split:
+        half = rows // 2
+        beside = (r + 1 - 2 * lax.rem(r, 2), lax.rem(r + 2, 4))
+        direct = {}
+
+        def forward(j):
+            for a in range(2):
+                direct[j, a].wait_recv()
+                block = block_of(j, beside[a], a * half, half)
+                c = remote(block, block, (s7, r7), (j, 2 + a), {"rep": beside[1 - a]})
+                c.start()
+                last.append(c)
+
     for j in range(F):
-        at = pl.multiple_of((back[j] * R + r) * rows, rows)
-        for i, ref in enumerate((qcopy_ref, vcopy_ref)):
+        if j > 0:
+            sixth[j - 1].wait_recv()
+        block = block_of(j, r, 0, rows)
+        if split:
+            for a in range(2):
+                direct[j, a] = remote(block, block, (s7, r7), (j, a), {"rep": beside[a]})
+                direct[j, a].start()
+                sends.append(direct[j, a])
             if j > 0:
-                sixth[(j - 1) * 2 + i].wait_recv()
-            block = ref.at[pl.ds(at, rows), :]
+                forward(j - 1)
+        else:
             for k in range(1, R):
-                c = remote(block, block, (s7, r7), (j, k * 2 + i), {"rep": rs[k]})
+                c = remote(block, block, (s7, r7), (j, k), {"rep": rs[k]})
                 c.start()
-                seventh.append(c)
-    sends += seventh
-    for c in seventh:
+                last.append(c)
+    if split:
+        forward(F - 1)
+    sends += last
+    for c in last:
         c.wait_recv()
     for c in sends:
         c.wait_send()
+
+
+def write_out(u, n, fn, sn, copy, qu, vu, qn, vn, qfn, qsn, vfn, vsn, qcopy, vcopy, sem):
+    QC, VC = qu.shape[1], vu.shape[1]
+    query, value = pl.ds(0, QC), pl.ds(QC, VC)
+    copies = [
+        pltpu.make_async_copy(src.at[:, part], dst, sem.at[i])
+        for i, (src, part, dst) in enumerate((
+            (copy, value, vcopy),
+            (copy, query, qcopy),
+            (u, value, vu),
+            (n, value, vn),
+            (u, query, qu),
+            (n, query, qn),
+            (fn, query, qfn),
+            (fn, value, vfn),
+            (sn, query, qsn),
+            (sn, value, vsn),
+        ))
+    ]
+    for c in copies:
+        c.start()
+    for c in copies:
+        c.wait()
 
 
 def fused(plain, *args):
@@ -303,9 +382,49 @@
     out = jax.ShapeDtypeStruct
     vmem = pl.BlockSpec(memory_space=pltpu.VMEM)
     dma = pltpu.SemaphoreType.DMA
+    results = pl.pallas_call(
+        functools.partial(kernel, F, R, T),
+        out_shape=[
+            pltpu.VMEM((rows, W), f32),
+            pltpu.VMEM((rows, W), f32),
+            pltpu.VMEM((M, W), f32),
+            pltpu.VMEM((M, W), f32),
+            pltpu.VMEM((rows * F * R, W), bf16),
+        ],
+        in_specs=[pl.BlockSpec(memory_space=pltpu.HBM)] * 11,
+        out_specs=[vmem] * 5,
+        scratch_shapes=[
+            pltpu.VMEM(x.shape, bf16),
+            pltpu.VMEM(qc.shape, bf16),
+            pltpu.VMEM(vc.shape, bf16),
+            pltpu.VMEM(qb.shape, bf16),
+            pltpu.VMEM(vb.shape, bf16),
+            pltpu.VMEM((rows, W), f32),
+            pltpu.VMEM((M, W), f32),
+            pltpu.VMEM((M, W), f32),
+            pltpu.VMEM((R, F, M, W), f32),
+            pltpu.VMEM((R, F, M, W), f32),
+            pltpu.VMEM((F, M, W), f32),
+            pltpu.VMEM((F, M, W), f32),
+            pltpu.VMEM((F, R, M, W), f32),
+            pltpu.VMEM((2, 8, 128), f32),
+            pltpu.VMEM((T, 2, 8, 128), f32),
+            dma((11,)),
+            dma((F, R)), dma((F, R)),
+            dma((F,)), dma((F,)),
+            dma((F,)), dma((F,)),
+            dma((F, R)), dma((F, R)),
+            dma((T,)), dma((T,)),
+            dma((F,)), dma((F,)),
+            dma((F, max(R, 4))), dma((F, max(R, 4))),
+        ],
+        compiler_params=pltpu.CompilerParams(
+            collective_id=0, has_side_effects=True, vmem_limit_bytes=VMEM_LIMIT
+        ),
+    )(*args)
     return tuple(
         pl.pallas_call(
-            functools.partial(kernel, F, R, T),
+            write_out,
             out_shape=[
                 out(qw.shape, f32),
                 out(vw.shape, f32),
@@ -318,28 +437,11 @@
                 out((rows * F * R, QC), bf16),
                 out((rows * F * R, VC), bf16),
             ],
-            in_specs=[vmem] * 11,
-            out_specs=[vmem] * 10,
-            scratch_shapes=[
-                pltpu.VMEM((R, F, M, W), f32),
-                pltpu.VMEM((R, F, M, W), f32),
-                pltpu.VMEM((F, M, W), f32),
-                pltpu.VMEM((F, M, W), f32),
-                pltpu.VMEM((F, R, M, W), f32),
-                pltpu.VMEM((2, 8, 128), f32),
-                pltpu.VMEM((T, 2, 8, 128), f32),
-                dma((R,)), dma((R,)),
-                dma((F,)), dma((F,)),
-                dma((F,)), dma((F,)),
-                dma((F, R)), dma((F, R)),
-                dma((T,)), dma((T,)),
-                dma((F, 2)), dma((F, 2)),
-                dma((F, 2 * R)), dma((F, 2 * R)),
-            ],
-            compiler_params=pltpu.CompilerParams(
-                collective_id=0, has_side_effects=True, vmem_limit_bytes=48 * 2**20
-            ),
-        )(*args)
+            in_specs=[vmem] * 5,
+            out_specs=[pl.BlockSpec(memory_space=pltpu.HBM)] * 10,
+            scratch_shapes=[dma((10,))],
+            compiler_params=pltpu.CompilerParams(vmem_limit_bytes=OUT_LIMIT),
+        )(*results)
     )
 
 

time: 62.5 us -> 46.3 us (0.74)
  local copies, waits for them, and re-layouts: 15.9 us -> 0 us
    unnamed x32 -> x0, local copies, waits for them, and re-layouts: 15.9 us -> none
    pallas_call x1 -> x2, Pallas kernels: 45.4 us -> 45.4 us  [the longest x1 44.1 us: fused(): pl.pallas_call(functools.partial(kernel, F, R, T), out_shape=[pltpu.VMEM(...]
where the time goes in v2:
time: 46.3 us; the launch traced here: 46.1 us
  Pallas kernels  45.4 us (98%)
  between operations  0.65 us (1%)
    pallas_call x1, Pallas kernels, fused(): pl.pallas_call(functools.partial(kernel, F, R, T), out_shape=[pltpu.VMEM(...  44.1 us
    pallas_call x1, Pallas kernels, fused(): pl.pallas_call(write_out, out_shape=[out(qw.shape, f32), out(vw.shape, f3...  1.36 us

profile of v2, /device:TPU:0, one launch (start us, length us, event | category | flops | bytes accessed | tf_op | source)
XLA Modules:
  0.0 46.1 jit_solution(1319602155400624607)
XLA Ops:
  0.6 44.1 %shard_map.186 = (f32[64,768]{1,0:T(8,128)S(1)}, f32[64,768]{1,0:T(8,128)S(1)}, f32[8,768]{1,0:T(8,128)S(1)}, f32[8,768]{1,0:T(8,128)S(1)}, bf16[1024,768]{1,0:T(8,128)(2,1)S(1)}) custom-call(bf16[128,1024]{1,0:T(8,128)(2,1)} %x_hbm.1, bf16[128,256]{1,0:T(8,128)(2,1)} %qc_hbm.1, bf16[128,512]{1,0:T(8,128)(2,1)} %vc_hbm.1, bf16[1024,128]{1,0:T(8,128)(2,1)} %qb_hbm.1, ...), custom_call_target="tpu_custom_call" | custom-call | tf_op jit(solution)/shard_map/pallas_call | solution.py:385
  44.7 1.4 %shard_map.187 = (f32[64,256]{1,0:T(8,128)}, f32[64,512]{1,0:T(8,128)}, f32[64,256]{1,0:T(8,128)}, f32[64,512]{1,0:T(8,128)}, f32[8,256]{1,0:T(8,128)}, /*index=...) custom-call(f32[64,768]{1,0:T(8,128)S(1)} %get-tuple-element.15.u, ...), custom_call_target="tpu_custom_call" | custom-call | tf_op jit(solution)/shard_map/pallas_call | solution.py:426

commit v3 on v2

--- a/solution.py
+++ b/solution.py
@@ -117,6 +117,10 @@
 
 
 MESH = pl.DeviceIdType.MESH
+ORDER = (1, 3, 2)
+EARLY_FS = 2
+REP_AT = 1
+SPLIT_EARLY = True
 VMEM_LIMIT = 60 * 2**20
 OUT_LIMIT = 16 * 2**20
 f32, bf16 = jnp.float32, jnp.bfloat16
@@ -149,15 +153,18 @@
     F, R, T,
     x_hbm, qc_hbm, vc_hbm, qb_hbm, vb_hbm, qw_hbm, vw_hbm, qf_hbm, qs_hbm, vf_hbm, vs_hbm,
     u_ref, n_ref, fn_ref, sn_ref, copy_ref,
-    x_ref, qc_ref, vc_ref, qb_ref, vb_ref, w_ref, f_ref, s_ref,
+    x_ref, qc_ref, vc_ref, qb_ref, vb_ref, w_ref, f_ref, s_ref, near_ref,
     part, got1, mid, got2, dirs, squares, squares_in,
-    load, s1, r1, s2, r2, s3, r3, s4, r4, s5, r5, s6, r6, s7, r7,
+    load, s1, r1, s2, r2, s3, r3, s4, r4, s5, r5, s6, r6, s7, r7, s8, r8, s9, r9,
 ):
     z, r, t = lax.axis_index("fs"), lax.axis_index("rep"), lax.axis_index("tp")
     zs = [lax.rem(z + k, F) for k in range(F)]
     rs = [lax.rem(r + k, R) for k in range(R)]
     ts = [lax.rem(t + k, T) for k in range(T)]
     back = [lax.rem(z + F - k, F) for k in range(F)]
+    if F == 4:
+        pairs = {1: z + 1 - 2 * lax.rem(z, 2), 2: lax.rem(z + 2, 4), 3: 3 - z}
+        zs = back = [z] + [pairs[k] for k in ORDER]
     rows = qw_hbm.shape[0]
     QC, VC = qc_hbm.shape[1], vc_hbm.shape[1]
     M = qf_hbm.shape[0]
@@ -208,6 +215,22 @@
     pl.semaphore_wait(barrier, F + R + T - 3)
 
     sends = []
+    rback = [lax.rem(r + R - k, R) for k in range(R)]
+    reach = min(EARLY_FS, F - 1)
+    middle_row = rows // 2 // 8 * 8 if SPLIT_EARLY else rows
+    tops = [(0, middle_row)] + ([(middle_row, rows)] if middle_row < rows else [])
+    near = {}
+    for k in range(1, reach + 1):
+        for i, (lo, hi) in enumerate(tops if k > 1 else [(0, rows)]):
+            near[k, i] = remote(
+                w_ref.at[lo:hi], near_ref.at[k - 1, lo:hi], (s8, r8), 2 * k + i, {"fs": zs[k]}
+            )
+    near_rep = [
+        remote(w_ref, near_ref.at[reach + k - 1], (s9, r9), k, {"rep": rs[k]})
+        for k in range(1, R)
+        if REP_AT
+    ]
+    sends += list(near.values()) + near_rep
     order = list(range(1, F)) + [0]
     first = {
         (j, k): remote(
@@ -219,6 +242,14 @@
     for c in first.values():
         c.start()
     sends += list(first.values())
+    for c in loads[9:]:
+        c.wait()
+    if REP_AT == 1:
+        for c in near_rep:
+            c.start()
+    for (k, i), c in near.items():
+        if i == 0:
+            c.start()
     second = {}
     for j in order:
         total = part[r, zs[j]]
@@ -230,7 +261,10 @@
             second[j] = remote(mid.at[j], got2.at[j], (s2, r2), j, {"fs": zs[j]})
             second[j].start()
     sends += list(second.values())
-    for c in loads[5:]:
+    if REP_AT == 2:
+        for c in near_rep:
+            c.start()
+    for c in loads[5:9]:
         c.wait()
     projected = total
     for j in range(1, F):
@@ -244,6 +278,9 @@
     third = [remote(dirs.at[z, r], dirs.at[z, r], (s3, r3), k, {"fs": zs[k]}) for k in range(1, F)]
     for c in third:
         c.start()
+    for (k, i), c in near.items():
+        if i == 1:
+            c.start()
     sends += third
     fourth = []
     for j in range(F):
@@ -275,70 +312,117 @@
     sends += fifth
 
     offset = pl.multiple_of((z * R + r) * rows, rows)
-    raw = []
-    for basis, start, width in ((qb_ref, 0, QC), (vb_ref, QC, VC)):
-        b = basis[pl.ds(offset, rows), :]
-        d1, d2, d3 = three_parts(whole[:, start : start + width])
-        raw.append(
-            jnp.dot(b, d1, preferred_element_type=f32)
-            + (jnp.dot(b, d2, preferred_element_type=f32) + jnp.dot(b, d3, preferred_element_type=f32))
-        )
+    split_dirs = [three_parts(whole[:, lo : lo + n]) for lo, n in ((0, QC), (QC, VC))]
+
+    def start_of(fs, rep):
+        return pl.multiple_of((fs * R + rep) * rows, rows)
+
+    def product(starts):
+        results = []
+        for basis, (d1, d2, d3) in zip((qb_ref, vb_ref), split_dirs):
+            b = jnp.concatenate([basis[pl.ds(at, rows), :] for at in starts], axis=0)
+            results.append(
+                jnp.dot(b, d1, preferred_element_type=f32)
+                + (
+                    jnp.dot(b, d2, preferred_element_type=f32)
+                    + jnp.dot(b, d3, preferred_element_type=f32)
+                )
+            )
+        return results
+
+    beyond = [start_of(back[k], r) for k in range(1, reach + 1)]
+    raw = product([offset] + beyond)
+    for c in near.values():
+        c.wait_recv()
     for c in fifth:
         c.wait_recv()
     sq = squares[...]
     for k in range(1, T):
         sq = sq + squares_in[k]
-    for i, (start, width) in enumerate(((0, QC), (QC, VC))):
-        scale = jnp.sqrt(jnp.sum(sq[i], keepdims=True) / (F * R * M * width * T) + 1.0)
-        update = raw[i] / scale
+    spans = ((0, QC), (QC, VC))
+    scales = [
+        jnp.sqrt(jnp.sum(sq[i], keepdims=True) / (F * R * M * width * T) + 1.0)
+        for i, (start, width) in enumerate(spans)
+    ]
+
+    def copy_rows(raw, first, starts, slot):
+        for i, (start, width) in enumerate(spans):
+            for n, at in enumerate(starts):
+                update = raw[i][(first + n) * rows : (first + n + 1) * rows] / scales[i]
+                new = near_ref[slot + n, :, start : start + width] - 0.01 * update
+                copy_ref[pl.ds(at, rows), start : start + width] = new.astype(bf16)
+
+    for i, (start, width) in enumerate(spans):
+        update = raw[i][:rows] / scales[i]
         new = w_ref[:, start : start + width] - 0.01 * update
         copy_ref[pl.ds(offset, rows), start : start + width] = new.astype(bf16)
         u_ref[:, start : start + width] = update
         n_ref[:, start : start + width] = new
-
-    own = copy_ref.at[pl.ds(offset, rows), :]
-    sixth = [remote(own, own, (s6, r6), k, {"fs": zs[k]}) for k in range(1, F)]
-    for c in sixth:
-        c.start()
-    sends += sixth
-
-    def block_of(j, rep, first_row, count):
-        at = pl.multiple_of((back[j] * R + rep) * rows + first_row, count)
-        return copy_ref.at[pl.ds(at, count), :]
+    copy_rows(raw, 1, beyond, 0)
+
+    parts = 2 if R == 4 and rows % 32 == 0 else 1
+    size = rows // parts
+
+    def piece(j, rep, p):
+        at = pl.multiple_of((back[j] * R + rep) * rows + p * size, size)
+        return copy_ref.at[pl.ds(at, size), :]
+
+    ready = 1 + reach
+    sixth = {}
+    for k in range(ready, F):
+        for p in range(parts):
+            own = piece(0, r, p)
+            sixth[k, p] = remote(own, own, (s6, r6), (k, p), {"fs": zs[k]})
+            sixth[k, p].start()
+    sends += list(sixth.values())
 
     last = []
-    split = R == 4 and rows % 32 == 0
-    if split:
-        half = rows // 2
-        beside = (r + 1 - 2 * lax.rem(r, 2), lax.rem(r + 2, 4))
-        direct = {}
-
-        def forward(j):
-            for a in range(2):
-                direct[j, a].wait_recv()
-                block = block_of(j, beside[a], a * half, half)
-                c = remote(block, block, (s7, r7), (j, 2 + a), {"rep": beside[1 - a]})
-                c.start()
-                last.append(c)
-
-    for j in range(F):
-        if j > 0:
-            sixth[j - 1].wait_recv()
-        block = block_of(j, r, 0, rows)
-        if split:
-            for a in range(2):
-                direct[j, a] = remote(block, block, (s7, r7), (j, a), {"rep": beside[a]})
-                direct[j, a].start()
-                sends.append(direct[j, a])
-            if j > 0:
-                forward(j - 1)
-        else:
-            for k in range(1, R):
-                c = remote(block, block, (s7, r7), (j, k), {"rep": rs[k]})
-                c.start()
-                last.append(c)
-    if split:
+    beside = (r + 1 - 2 * lax.rem(r, 2), lax.rem(r + 2, 4))
+    direct = {}
+
+    def forward(j):
+        for a in range(2):
+            direct[j, a, a].wait_recv()
+            block = piece(j, beside[a], a)
+            c = remote(block, block, (s7, r7), (j, 4 + a), {"rep": beside[1 - a]})
+            c.start()
+            last.append(c)
+
+    first_block = 1 if REP_AT else 0
+    for j in range(first_block, F):
+        if REP_AT and j == min(ready, F - 1):
+            beside_rows = [start_of(z, rback[k]) for k in range(1, R)]
+            raw = product(beside_rows)
+            for c in near_rep:
+                c.wait_recv()
+            copy_rows(raw, 0, beside_rows, reach)
+        for p in range(parts):
+            if j >= ready:
+                sixth[j, p].wait_recv()
+            if parts == 1:
+                for k in range(1, R):
+                    block = piece(j, r, 0)
+                    c = remote(block, block, (s7, r7), (j, k), {"rep": rs[k]})
+                    c.start()
+                    last.append(c)
+            elif j >= ready:
+                for a in (p, 1 - p):
+                    block = piece(j, r, p)
+                    direct[j, a, p] = remote(block, block, (s7, r7), (j, a * 2 + p), {"rep": beside[a]})
+                    direct[j, a, p].start()
+        if parts == 2 and j < ready:
+            for a, p in ((0, 0), (1, 1), (0, 1), (1, 0)):
+                block = piece(j, r, p)
+                direct[j, a, p] = remote(block, block, (s7, r7), (j, a * 2 + p), {"rep": beside[a]})
+                direct[j, a, p].start()
+        if parts == 2 and j > first_block:
+            forward(j - 1)
+    if parts == 2:
         forward(F - 1)
+    for (j, a, p), c in direct.items():
+        if a != p:
+            c.wait_recv()
+        sends.append(c)
     sends += last
     for c in last:
         c.wait_recv()
@@ -402,6 +486,7 @@
             pltpu.VMEM((rows, W), f32),
             pltpu.VMEM((M, W), f32),
             pltpu.VMEM((M, W), f32),
+            pltpu.VMEM((min(EARLY_FS, F - 1) + R - 1, rows, W), f32),
             pltpu.VMEM((R, F, M, W), f32),
             pltpu.VMEM((R, F, M, W), f32),
             pltpu.VMEM((F, M, W), f32),
@@ -415,8 +500,10 @@
             dma((F,)), dma((F,)),
             dma((F, R)), dma((F, R)),
             dma((T,)), dma((T,)),
-            dma((F,)), dma((F,)),
-            dma((F, max(R, 4))), dma((F, max(R, 4))),
+            dma((F, 2)), dma((F, 2)),
+            dma((F, max(R, 6))), dma((F, max(R, 6))),
+            dma((2 * F,)), dma((2 * F,)),
+            dma((R,)), dma((R,)),
         ],
         compiler_params=pltpu.CompilerParams(
             collective_id=0, has_side_effects=True, vmem_limit_bytes=VMEM_LIMIT

time: 46.3 us -> 43.4 us (0.937)
  Pallas kernels: 45.4 us -> 42.6 us
    pallas_call x1, Pallas kernels: 44.1 us -> 41.2 us  [fused(): pl.pallas_call(functools.partial(kernel, F, R, T), out_shape=[pltpu.VMEM(...]
where the time goes in v3:
time: 43.4 us; the launch traced here: 43.2 us
  Pallas kernels  42.6 us (98%)
  between operations  0.65 us (1%)
    pallas_call x1, Pallas kernels, fused(): pl.pallas_call(functools.partial(kernel, F, R, T), out_shape=[pltpu.VMEM(...  41.2 us
    pallas_call x1, Pallas kernels, fused(): pl.pallas_call(write_out, out_shape=[out(qw.shape, f32), out(vw.shape, f3...  1.36 us

profile of v3, /device:TPU:0, one launch (start us, length us, event | category | flops | bytes accessed | tf_op | source)
XLA Modules:
  0.0 43.2 jit_solution(3621339210866745434)
XLA Ops:
  0.6 41.2 %shard_map.186 = (f32[64,768]{1,0:T(8,128)S(1)}, f32[64,768]{1,0:T(8,128)S(1)}, f32[8,768]{1,0:T(8,128)S(1)}, f32[8,768]{1,0:T(8,128)S(1)}, bf16[1024,768]{1,0:T(8,128)(2,1)S(1)}) custom-call(bf16[128,1024]{1,0:T(8,128)(2,1)} %x_hbm.1, bf16[128,256]{1,0:T(8,128)(2,1)} %qc_hbm.1, bf16[128,512]{1,0:T(8,128)(2,1)} %vc_hbm.1, bf16[1024,128]{1,0:T(8,128)(2,1)} %qb_hbm.1, ...), custom_call_target="tpu_custom_call" | custom-call | tf_op jit(solution)/shard_map/pallas_call | solution.py:469
  41.9 1.4 %shard_map.187 = (f32[64,256]{1,0:T(8,128)}, f32[64,512]{1,0:T(8,128)}, f32[64,256]{1,0:T(8,128)}, f32[64,512]{1,0:T(8,128)}, f32[8,256]{1,0:T(8,128)}, /*index=...) custom-call(f32[64,768]{1,0:T(8,128)S(1)} %get-tuple-element.15.u, ...), custom_call_target="tpu_custom_call" | custom-call | tf_op jit(solution)/shard_map/pallas_call | solution.py:513
